TPU v7x, 32 devices: a whole 2x2x4 slice. The times are simulated.
32 devices in a mesh: ra: 16 (over z, y, x), cb: 2 (over core).
Axes of the slice: x: 2, y: 2, z: 4, core: 2. Of those that a mesh axis runs over, the one named last changes fastest.
Arguments:
- activations: bfloat16 [768, 4096], P('ra', 'cb'), may hold values from -230 to 230
- gain_first: float32 [4096], P('cb'), may hold values from 0.1 to 1.9
- gate_weight: float32 [11264, 4096], P('ra', 'cb'), may hold values from -0.125 to 0.125
- gate_scale: float32 [11264], P('ra'), may hold values from 0.5 to 2
- up_weight: float32 [11264, 4096], P('ra', 'cb'), may hold values from -0.125 to 0.125
- up_scale: float32 [11264], P('ra'), may hold values from 0.5 to 2
- down_weight: float32 [11264, 4096], P('ra', 'cb'), may hold values from -0.0546875 to 0.0546875
- down_scale: float32 [4096], P('cb'), may hold values from 0.35 to 2.8
- gain_second: float32 [4096], P('cb'), may hold values from 0.1 to 1.9
Outputs:
- normed: bfloat16 [768, 4096], P('ra', 'cb')
All inputs are finite; a program needn't handle non-finite values.
Results may differ from a plain program's by a relative error of at most 0.011.
Values may be sent and summed in bfloat16 or wider, within the bound.
A program may use at most 64 MiB of HBM per device.

v0:
```python
import jax
import jax.numpy as jnp
from jax import lax
from jax.sharding import PartitionSpec as P

EPS = 1e-06


def per_device(
    activations,
    gain_first,
    gate_weight,
    gate_scale,
    up_weight,
    up_scale,
    down_weight,
    down_scale,
    gain_second,
):
    inputs = activations.astype(jnp.float32)
    features = activations.shape[1] * lax.axis_size("cb")
    gate_local = gate_weight.astype(jnp.bfloat16)
    up_local = up_weight.astype(jnp.bfloat16)
    down_local = down_weight.astype(jnp.bfloat16)
    gathered = lax.all_gather(activations, "ra", axis=0, tiled=True)
    wide_rows = gathered.astype(jnp.float32)
    row_squares = jnp.sum(wide_rows * wide_rows, axis=1)
    scaled = (wide_rows * gain_first).astype(jnp.bfloat16)
    contract = (((1,), (1,)), ((), ()))
    squares = lax.psum(row_squares, "cb")
    gate_part = lax.dot_general(gate_local, scaled, contract, preferred_element_type=jnp.float32)
    up_part = lax.dot_general(up_local, scaled, contract, preferred_element_type=jnp.float32)
    gate_sum, up_sum = lax.psum((gate_part, up_part), "cb")
    rscale_first = lax.rsqrt(squares / features + EPS)[None, :]
    gate_full = gate_sum * rscale_first * gate_scale[:, None]
    up_full = up_sum * rscale_first * up_scale[:, None]
    hidden = (jax.nn.silu(gate_full) * up_full).astype(jnp.bfloat16)
    summed = lax.psum_scatter(
        lax.dot_general(
            hidden, down_local, (((0,), (0,)), ((), ())), preferred_element_type=jnp.float32
        ),
        "ra",
        scatter_dimension=0,
        tiled=True,
    )
    stream = 0.1 * inputs + summed * down_scale
    second = lax.psum(jnp.sum(stream * stream, axis=1), "cb")
    rscale_second = lax.rsqrt(second / features + EPS)[:, None]
    return (stream * rscale_second * gain_second).astype(jnp.bfloat16)


def solution(mesh):
    placed = (
        P("ra", "cb"),
        P("cb"),
        P("ra", "cb"),
        P("ra"),
        P("ra", "cb"),
        P("ra"),
        P("ra", "cb"),
        P("cb"),
        P("cb"),
    )
    return jax.shard_map(
        per_device, mesh=mesh, in_specs=placed, out_specs=P("ra", "cb"), check_vma=False
    )
```

profile of v0, /device:TPU:0, one launch (start us, length us, event | category | flops | bytes accessed | tf_op | source)
XLA Modules:
  0.0 292.0 jit_solution(9927717845892913069)
XLA Ops:
  6.5 0.0 all-gather.2.cloned.1.call-start
  6.5 0.7 all-gather.2.cloned.1.call-update
  7.3 0.0 copy-start.4
  7.3 0.0 all-reduce.3.cloned.1.call-start
  7.3 73.4 %all-gather.2.cloned.1.call-done = bf16[768,2048]{1,0:T(8,128)(2,1)} async-done(((bf16[48,2048]{1,0:T(8,128)(2,1)}), bf16[768,2048]{1,0:T(8,128)(2,1)}) %all-gather.2.cloned.1.call-update) | async-done | bytes 3145744 | tf_op jit(solution)/shard_map/all_gather | solution.py:25
  80.7 0.0 copy-start
  80.7 7.5 %fusion.15 = f32[704,768]{1,0:T(8,128)} fusion(f32[704,2048]{1,0:T(8,128)} %param.13, bf16[768,2048]{1,0:T(8,128)(2,1)} %all-gather.2.cloned.1.call-done, f32[2048]{0:T(1024)} %param.10), kind=kOutput, calls=%fused_computation.12 | convolution fusion | flops 2220752896 | bytes 11083776 | tf_op jit(solution)/shard_map/dot_general | solution.py:32
  88.3 0.0 copy-done.4
  88.3 0.0 copy-done
  88.3 6.4 %fusion.10 = f32[704,768]{1,0:T(8,128)} fusion(f32[704,2048]{1,0:T(8,128)} %param.11, bf16[768,2048]{1,0:T(8,128)(2,1)S(1)} %copy-done, f32[2048]{0:T(1024)S(1)} %copy-done.4), kind=kOutput, calls=%fused_computation.11 | convolution fusion | flops 2220752896 | bytes 11083776 | tf_op jit(solution)/shard_map/dot_general | solution.py:31
  94.7 0.0 copy-start.5
  94.7 0.0 copy-start.6
  94.7 0.0 all-reduce.3.cloned.1.call-update
  94.7 0.0 reduce-scatter.2.cloned.1.call-start
  94.8 0.7 fusion.1
  95.5 2.5 psum.29
  97.9 23.9 %all-reduce.3.cloned.1.call-done = (f32[704,768]{1,0:T(8,128)}, f32[704,768]{1,0:T(8,128)}) async-done(((f32[704,768]{1,0:T(8,128)}, f32[704,768]{1,0:T(8,128)}), (f32[704,768]{1,0:T(8,128)}, f32[704,768]{1,0:T(8,128)})) %all-reduce.3.cloned.1.call-update) | async-done | bytes 4325392 | tf_op jit(solution)/shard_map/psum | solution.py:33
  121.9 0.0 copy-done.5
  121.9 0.0 copy-done.6
  121.9 9.5 %fusion.2 = f32[768,2048]{1,0:T(8,128)} fusion(f32[704,2048]{1,0:T(8,128)} %param.15, f32[704,768]{1,0:T(8,128)} %get-tuple-element.5, f32[704,768]{1,0:T(8,128)} %get-tuple-element.6, f32[704]{0:T(1024)S(1)} %copy-done.5, f32[704]{0:T(1024)S(1)} %copy-done.6, f32[768]{0:T(1024)S(1)} %add_rsqrt_fusion), kind=kOutput, calls=%fused_computation.4 | convolution fusion | flops 2221441024 | bytes 16392704 | tf_op jit(solution)/shard_map/dot_general | solution.py:39
  131.3 0.0 copy-start.1
  131.3 0.0 copy-start.2
  131.4 0.0 copy-start.3
  131.4 0.0 reduce-scatter.2.cloned.1.call-update
  131.4 148.7 %reduce-scatter.2.cloned.1.call-done = f32[48,2048]{1,0:T(8,128)} async-done(((f32[768,2048]{1,0:T(8,128)}), f32[48,2048]{1,0:T(8,128)}) %reduce-scatter.2.cloned.1.call-update) | async-done | bytes 393232 | tf_op jit(solution)/shard_map/reduce_scatter | solution.py:38
  280.1 0.0 copy-done.1
  280.1 0.0 copy-done.2
  280.1 1.2 multiply_reduce_fusion
  281.2 2.5 psum.31
  283.7 0.0 copy-done.3
  283.7 1.8 multiply_convert_fusion.2
  (2 shorter events, 0.0 us)
Async XLA Ops:
  6.5 74.2 %all-gather.2.cloned.1.call-start = ((), (), s32[]{:S(2)}) async-start(), calls=%async_computation.1 | async-start | bytes 3342336 | tf_op jit(solution)/shard_map/all_gather | solution.py:25
  7.3 81.0 %copy-start.4 = (f32[2048]{0:T(1024)S(1)}, f32[2048]{0:T(1024)}, u32[]{:S(2)}) copy-start(f32[2048]{0:T(1024)} %param.10) | copy-start | bytes 24580
  7.3 114.6 %all-reduce.3.cloned.1.call-start = ((), (), s32[]{:S(2)}) async-start(), calls=%async_computation.3 | async-start | bytes 8650752 | tf_op jit(solution)/shard_map/psum | solution.py:33
  80.7 7.6 %copy-start = (bf16[768,2048]{1,0:T(8,128)(2,1)S(1)}, bf16[768,2048]{1,0:T(8,128)(2,1)}, u32[]{:S(2)}) copy-start(bf16[768,2048]{1,0:T(8,128)(2,1)} %all-gather.2.cloned.1.call-done) | copy-start | bytes 9437188
  94.7 27.2 %copy-start.5 = (f32[704]{0:T(1024)S(1)}, f32[704]{0:T(1024)}, u32[]{:S(2)}) copy-start(f32[704]{0:T(1024)} %param.14) | copy-start | bytes 8452
  94.7 27.2 %copy-start.6 = (f32[704]{0:T(1024)S(1)}, f32[704]{0:T(1024)}, u32[]{:S(2)}) copy-start(f32[704]{0:T(1024)} %param.12) | copy-start | bytes 8452
  94.7 185.3 %reduce-scatter.2.cloned.1.call-start = ((), (), s32[]{:S(2)}) async-start(), calls=%async_computation.2 | async-start | bytes 6684672 | tf_op jit(solution)/shard_map/reduce_scatter | solution.py:38
  131.3 148.7 %copy-start.1 = (bf16[48,2048]{1,0:T(8,128)(2,1)S(1)}, bf16[48,2048]{1,0:T(8,128)(2,1)}, u32[]{:S(2)}) copy-start(bf16[48,2048]{1,0:T(8,128)(2,1)} %param.9) | copy-start | bytes 589828
  131.3 148.7 %copy-start.2 = (f32[2048]{0:T(1024)S(1)}, f32[2048]{0:T(1024)}, u32[]{:S(2)}) copy-start(f32[2048]{0:T(1024)} %param.16) | copy-start | bytes 24580
  131.4 152.4 %copy-start.3 = (f32[2048]{0:T(1024)S(1)}, f32[2048]{0:T(1024)}, u32[]{:S(2)}) copy-start(f32[2048]{0:T(1024)} %param.17) | copy-start | bytes 24580
Sparse Core Ops, SparseCore 0:
  10.1 70.5 all-gather.1
  94.9 26.9 all-reduce.2
  131.5 148.5 reduce-scatter.1
where the time goes:
time: 292 us
  waiting for transfers between devices  247 us (85%)
  matrix products  23.4 us (8%)
  between operations  13.1 us (4%)
  blocking collectives  4.95 us (2%)
  other arithmetic  3.66 us (1%)
    reduce_scatter x1, waiting for transfers between devices, per_device(): lax.psum_scatter(lax.dot_general(hidden, down_local, (((0,), (0,)), ((),...  149 us
    all_gather x1, waiting for transfers between devices, per_device(): gathered = lax.all_gather(activations, 'ra', axis=0, tiled=True)  73.4 us
    psum x1, waiting for transfers between devices, per_device(): gate_sum, up_sum = lax.psum((gate_part, up_part), 'cb')  23.9 us
    dot_general x1, matrix products, per_device(): lax.dot_general(hidden, down_local, (((0,), (0,)), ((), ())), preferred_e...  9.48 us
    dot_general x1, matrix products, per_device(): lax.dot_general(up_local, scaled, contract, preferred_element_type=jnp.fl...  7.55 us
    dot_general x1, matrix products, per_device(): lax.dot_general(gate_local, scaled, contract, preferred_element_type=jnp....  6.42 us
  transfers between devices with their start and end apart: 3, of which 3 were waited for; matrix products, arithmetic and copies ran while one was open for 0% of the time, Pallas kernels for 0%

commit v1 on v0

--- a/solution.py
+++ b/solution.py
@@ -4,6 +4,22 @@
 from jax.sharding import PartitionSpec as P
 
 EPS = 1e-06
+
+
+def review_the_pools(m, row_axis):
+    sides = lax.axis_size(row_axis)
+    grid = []
+    for dev_i in range(sides):
+        grid.append((dev_i, (dev_i + 1) % sides))
+    local_next = [None] * sides
+    local_next[sides - 1] = m
+    for dev in range(sides - 2, -1, -1):
+        local_next[dev] = lax.ppermute(local_next[dev + 1], axis_name=row_axis, perm=grid)
+    return jnp.roll(
+        jnp.concatenate(local_next, axis=0),
+        shift=(lax.axis_index(row_axis) + 1) * m.shape[0],
+        axis=0,
+    )
 
 
 def per_device(
@@ -22,7 +38,7 @@
     gate_local = gate_weight.astype(jnp.bfloat16)
     up_local = up_weight.astype(jnp.bfloat16)
     down_local = down_weight.astype(jnp.bfloat16)
-    gathered = lax.all_gather(activations, "ra", axis=0, tiled=True)
+    gathered = review_the_pools(activations, "ra")
     wide_rows = gathered.astype(jnp.float32)
     row_squares = jnp.sum(wide_rows * wide_rows, axis=1)
     scaled = (wide_rows * gain_first).astype(jnp.bfloat16)

time: 292 us -> 359 us (1.23)
  waiting for transfers between devices: 247 us -> 310 us
  matrix products: 23.4 us -> 17.1 us
    ppermute x0 -> x15, waiting for transfers between devices: none -> 144 us  [review_the_pools(): lax.ppermute(local_next[dev + 1], axis_name=row_axis, perm=grid)]
    all_gather x1 -> x0, waiting for transfers between devices: 73.4 us -> none  [per_device(): gathered = lax.all_gather(activations, 'ra', axis=0, tiled=True)]
    psum x1, waiting for transfers between devices: 23.9 us -> 18.7 us  [per_device(): gate_sum, up_sum = lax.psum((gate_part, up_part), 'cb')]
    dot_general x1, matrix products: 7.55 us -> 3.83 us  [per_device(): lax.dot_general(up_local, scaled, contract, preferred_element_type=jnp.fl...]
  transfers between devices with their start and end apart: 3 -> 17, of which waited for: 3 -> 17; matrix products, arithmetic and copies ran while one was open for 0% -> 1% of each run, Pallas kernels for 0% -> 0%
where the time goes in v1:
time: 359 us
  waiting for transfers between devices  310 us (86%)
  matrix products  17.1 us (5%)
  between operations  13.7 us (4%)
  other arithmetic  6.2 us (2%)
  blocking collectives  4.94 us (1%)
    reduce_scatter x1, waiting for transfers between devices, per_device(): lax.psum_scatter(lax.dot_general(hidden, down_local, (((0,), (0,)), ((),...  148 us
    ppermute x15, waiting for transfers between devices, review_the_pools(): lax.ppermute(local_next[dev + 1], axis_name=row_axis, perm=grid)  144 us
    psum x1, waiting for transfers between devices, per_device(): gate_sum, up_sum = lax.psum((gate_part, up_part), 'cb')  18.7 us
    dot_general x1, matrix products, per_device(): lax.dot_general(hidden, down_local, (((0,), (0,)), ((), ())), preferred_e...  9.49 us
  transfers between devices with their start and end apart: 17, of which 17 were waited for; matrix products, arithmetic and copies ran while one was open for 1% of the time, Pallas kernels for 0%

profile of v1, /device:TPU:0, one launch (start us, length us, event | category | flops | bytes accessed | tf_op | source)
XLA Modules:
  0.0 358.7 jit_solution(11883989351126041309)
XLA Ops:
  6.5 0.0 copy-start
  6.5 0.0 all-reduce.3.cloned.1.call-start
  6.5 3.0 collective-permute-start
  9.5 9.2 %collective-permute-done = bf16[48,2048]{1,0:T(8,128)(2,1)S(1)} collective-permute-done((bf16[48,2048]{1,0:T(8,128)(2,1)}, bf16[48,2048]{1,0:T(8,128)(2,1)S(1)}, u32[]{:S(2)}, u32[]{:S(2)}) %collective-permute-start) | collective-permute-done | bytes 196640 | tf_op jit(solution)/shard_map/ppermute | solution.py:17
  18.7 0.0 collective-permute-start.1
  18.7 9.7 %collective-permute-done.1 = bf16[48,2048]{1,0:T(8,128)(2,1)S(1)} collective-permute-done((bf16[48,2048]{1,0:T(8,128)(2,1)S(1)}, bf16[48,2048]{1,0:T(8,128)(2,1)S(1)}, u32[]{:S(2)}, u32[]{:S(2)}) %collective-permute-start.1) | collective-permute-done | bytes 196640 | tf_op jit(solution)/shard_map/ppermute | solution.py:17
  28.3 0.0 collective-permute-start.2
  28.3 9.3 %collective-permute-done.2 = bf16[48,2048]{1,0:T(8,128)(2,1)S(1)} collective-permute-done((bf16[48,2048]{1,0:T(8,128)(2,1)S(1)}, bf16[48,2048]{1,0:T(8,128)(2,1)S(1)}, u32[]{:S(2)}, u32[]{:S(2)}) %collective-permute-start.2) | collective-permute-done | bytes 196640 | tf_op jit(solution)/shard_map/ppermute | solution.py:17
  37.6 0.0 collective-permute-start.3
  37.6 9.3 %collective-permute-done.3 = bf16[48,2048]{1,0:T(8,128)(2,1)S(1)} collective-permute-done((bf16[48,2048]{1,0:T(8,128)(2,1)S(1)}, bf16[48,2048]{1,0:T(8,128)(2,1)S(1)}, u32[]{:S(2)}, u32[]{:S(2)}) %collective-permute-start.3) | collective-permute-done | bytes 196640 | tf_op jit(solution)/shard_map/ppermute | solution.py:17
  46.9 0.0 collective-permute-start.4
  46.9 9.3 %collective-permute-done.4 = bf16[48,2048]{1,0:T(8,128)(2,1)S(1)} collective-permute-done((bf16[48,2048]{1,0:T(8,128)(2,1)S(1)}, bf16[48,2048]{1,0:T(8,128)(2,1)S(1)}, u32[]{:S(2)}, u32[]{:S(2)}) %collective-permute-start.4) | collective-permute-done | bytes 196640 | tf_op jit(solution)/shard_map/ppermute | solution.py:17
  56.1 0.0 collective-permute-start.5
  56.1 9.3 %collective-permute-done.5 = bf16[48,2048]{1,0:T(8,128)(2,1)S(1)} collective-permute-done((bf16[48,2048]{1,0:T(8,128)(2,1)S(1)}, bf16[48,2048]{1,0:T(8,128)(2,1)S(1)}, u32[]{:S(2)}, u32[]{:S(2)}) %collective-permute-start.5) | collective-permute-done | bytes 196640 | tf_op jit(solution)/shard_map/ppermute | solution.py:17
  65.4 0.0 collective-permute-start.6
  65.4 10.4 %collective-permute-done.6 = bf16[48,2048]{1,0:T(8,128)(2,1)S(1)} collective-permute-done((bf16[48,2048]{1,0:T(8,128)(2,1)S(1)}, bf16[48,2048]{1,0:T(8,128)(2,1)S(1)}, u32[]{:S(2)}, u32[]{:S(2)}) %collective-permute-start.6) | collective-permute-done | bytes 196640 | tf_op jit(solution)/shard_map/ppermute | solution.py:17
  75.8 0.0 collective-permute-start.7
  75.8 11.2 %collective-permute-done.7 = bf16[48,2048]{1,0:T(8,128)(2,1)S(1)} collective-permute-done((bf16[48,2048]{1,0:T(8,128)(2,1)S(1)}, bf16[48,2048]{1,0:T(8,128)(2,1)S(1)}, u32[]{:S(2)}, u32[]{:S(2)}) %collective-permute-start.7) | collective-permute-done | bytes 196640 | tf_op jit(solution)/shard_map/ppermute | solution.py:17
  87.0 0.0 collective-permute-start.8
  87.0 10.3 %collective-permute-done.8 = bf16[48,2048]{1,0:T(8,128)(2,1)S(1)} collective-permute-done((bf16[48,2048]{1,0:T(8,128)(2,1)S(1)}, bf16[48,2048]{1,0:T(8,128)(2,1)S(1)}, u32[]{:S(2)}, u32[]{:S(2)}) %collective-permute-start.8) | collective-permute-done | bytes 196640 | tf_op jit(solution)/shard_map/ppermute | solution.py:17
  97.3 0.0 collective-permute-start.9
  97.3 9.5 %collective-permute-done.9 = bf16[48,2048]{1,0:T(8,128)(2,1)S(1)} collective-permute-done((bf16[48,2048]{1,0:T(8,128)(2,1)S(1)}, bf16[48,2048]{1,0:T(8,128)(2,1)S(1)}, u32[]{:S(2)}, u32[]{:S(2)}) %collective-permute-start.9) | collective-permute-done | bytes 196640 | tf_op jit(solution)/shard_map/ppermute | solution.py:17
  106.8 0.0 collective-permute-start.10
  106.8 9.3 %collective-permute-done.10 = bf16[48,2048]{1,0:T(8,128)(2,1)S(1)} collective-permute-done((bf16[48,2048]{1,0:T(8,128)(2,1)S(1)}, bf16[48,2048]{1,0:T(8,128)(2,1)S(1)}, u32[]{:S(2)}, u32[]{:S(2)}) %collective-permute-start.10) | collective-permute-done | bytes 196640 | tf_op jit(solution)/shard_map/ppermute | solution.py:17
  116.1 0.0 collective-permute-start.11
  116.1 9.3 %collective-permute-done.11 = bf16[48,2048]{1,0:T(8,128)(2,1)S(1)} collective-permute-done((bf16[48,2048]{1,0:T(8,128)(2,1)S(1)}, bf16[48,2048]{1,0:T(8,128)(2,1)S(1)}, u32[]{:S(2)}, u32[]{:S(2)}) %collective-permute-start.11) | collective-permute-done | bytes 196640 | tf_op jit(solution)/shard_map/ppermute | solution.py:17
  125.3 0.0 collective-permute-start.12
  125.3 9.3 %collective-permute-done.12 = bf16[48,2048]{1,0:T(8,128)(2,1)S(1)} collective-permute-done((bf16[48,2048]{1,0:T(8,128)(2,1)S(1)}, bf16[48,2048]{1,0:T(8,128)(2,1)S(1)}, u32[]{:S(2)}, u32[]{:S(2)}) %collective-permute-start.12) | collective-permute-done | bytes 196640 | tf_op jit(solution)/shard_map/ppermute | solution.py:17
  134.6 0.0 collective-permute-start.13
  134.6 9.3 %collective-permute-done.13 = bf16[48,2048]{1,0:T(8,128)(2,1)S(1)} collective-permute-done((bf16[48,2048]{1,0:T(8,128)(2,1)S(1)}, bf16[48,2048]{1,0:T(8,128)(2,1)S(1)}, u32[]{:S(2)}, u32[]{:S(2)}) %collective-permute-start.13) | collective-permute-done | bytes 196640 | tf_op jit(solution)/shard_map/ppermute | solution.py:17
  143.9 0.0 collective-permute-start.14
  143.9 0.0 copy-start.4
  143.9 0.0 copy-start.5
  143.9 9.3 %collective-permute-done.14 = bf16[48,2048]{1,0:T(8,128)(2,1)S(1)} collective-permute-done((bf16[48,2048]{1,0:T(8,128)(2,1)S(1)}, bf16[48,2048]{1,0:T(8,128)(2,1)S(1)}, u32[]{:S(2)}, u32[]{:S(2)}) %collective-permute-start.14) | collective-permute-done | bytes 196640 | tf_op jit(solution)/shard_map/ppermute | solution.py:17
  153.5 0.9 constant_dynamic-update-slice_fusion.16
  154.8 0.0 copy-done
  154.8 0.0 slice-start
  154.8 0.0 copy-done.4
  154.8 0.0 copy-done.5
  154.8 0.0 copy-start.1
  154.8 0.0 slice-start.1
  154.9 3.8 %fusion.10 = f32[704,768]{1,0:T(8,128)} fusion(f32[704,2048]{1,0:T(8,128)S(1)} %copy-done.4, f32[2048]{0:T(1024)S(1)} %copy-done.5, bf16[1536,2048]{1,0:T(8,128)(2,1)S(1)} %constant_dynamic-update-slice_fusion, s32[]{:T(128)S(6)} %select_n.14), kind=kOutput, calls=%fused_computation.11 | convolution fusion | flops 2220752896 | bytes 11083780 | tf_op jit(solution)/shard_map/dot_general | solution.py:47
  158.7 0.4 copy-done.1
  159.1 0.8 slice-done
  159.9 0.5 slice-done.1
  160.4 3.8 %fusion.15 = f32[704,768]{1,0:T(8,128)} fusion(f32[704,2048]{1,0:T(8,128)S(1)} %bitcast.5, f32[2048]{0:T(1024)S(1)} %copy-done.5, bf16[1536,2048]{1,0:T(8,128)(2,1)S(1)} %constant_dynamic-update-slice_fusion, s32[]{:T(128)S(6)} %select_n.14), kind=kOutput, calls=%fused_computation.12 | convolution fusion | flops 2220752896 | bytes 11083780 | tf_op jit(solution)/shard_map/dot_general | solution.py:48
  164.3 0.0 copy-start.6
  164.3 0.0 copy-start.7
  164.3 0.0 all-reduce.3.cloned.1.call-update
  164.3 0.0 reduce-scatter.2.cloned.1.call-start
  164.4 3.2 fusion.1
  167.6 2.5 psum.29
  170.1 18.7 %all-reduce.3.cloned.1.call-done = (f32[704,768]{1,0:T(8,128)}, f32[704,768]{1,0:T(8,128)}) async-done(((f32[704,768]{1,0:T(8,128)}, f32[704,768]{1,0:T(8,128)}), (f32[704,768]{1,0:T(8,128)}, f32[704,768]{1,0:T(8,128)})) %all-reduce.3.cloned.1.call-update) | async-done | bytes 4325392 | tf_op jit(solution)/shard_map/psum | solution.py:49
  188.7 0.0 copy-done.6
  188.7 0.0 copy-done.7
  188.7 9.5 %fusion.2 = f32[768,2048]{1,0:T(8,128)} fusion(f32[704,2048]{1,0:T(8,128)} %param.15, f32[704,768]{1,0:T(8,128)} %get-tuple-element.5, f32[704,768]{1,0:T(8,128)} %get-tuple-element.6, f32[704]{0:T(1024)S(1)} %copy-done.6, f32[704]{0:T(1024)S(1)} %copy-done.7, f32[768]{0:T(1024)S(1)} %add_rsqrt_fusion), kind=kOutput, calls=%fused_computation.4 | convolution fusion | flops 2221441024 | bytes 16392704 | tf_op jit(solution)/shard_map/dot_general | solution.py:55
  198.2 0.0 copy-start.2
  198.2 0.0 reduce-scatter.2.cloned.1.call-update
  198.3 148.2 %reduce-scatter.2.cloned.1.call-done = f32[48,2048]{1,0:T(8,128)} async-done(((f32[768,2048]{1,0:T(8,128)}), f32[48,2048]{1,0:T(8,128)}) %reduce-scatter.2.cloned.1.call-update) | async-done | bytes 393232 | tf_op jit(solution)/shard_map/reduce_scatter | solution.py:54
  346.4 0.0 copy-done.2
  346.4 1.2 multiply_reduce_fusion
  347.6 2.5 psum.31
  350.1 0.0 copy-done.3
  350.1 1.8 multiply_convert_fusion.2
  (35 shorter events, 0.5 us)
Async XLA Ops:
  6.5 148.2 %copy-start = (bf16[48,2048]{1,0:T(8,128)(2,1)S(1)}, bf16[48,2048]{1,0:T(8,128)(2,1)}, u32[]{:S(2)}) copy-start(bf16[48,2048]{1,0:T(8,128)(2,1)} %param.9) | copy-start | bytes 589828
  6.5 182.2 %all-reduce.3.cloned.1.call-start = ((), (), s32[]{:S(2)}) async-start(), calls=%async_computation.2 | async-start | bytes 8650752 | tf_op jit(solution)/shard_map/psum | solution.py:49
  6.5 12.1 %collective-permute-start = (bf16[48,2048]{1,0:T(8,128)(2,1)}, bf16[48,2048]{1,0:T(8,128)(2,1)S(1)}, u32[]{:S(2)}, u32[]{:S(2)}) collective-permute-start(bf16[48,2048]{1,0:T(8,128)(2,1)} %param.9), channel_id=1, source_target_pairs={{0,2},{2,4},{4,6},{6,8},{8,10},{10,12},{12,14},{14,16},{16,18},{18... | collective-permute-start | bytes 589832 | tf_op jit(solution)/shard_map/ppermute | solution.py:17
  18.7 9.7 %collective-permute-start.1 = (bf16[48,2048]{1,0:T(8,128)(2,1)S(1)}, bf16[48,2048]{1,0:T(8,128)(2,1)S(1)}, u32[]{:S(2)}, u32[]{:S(2)}) collective-permute-start(bf16[48,2048]{1,0:T(8,128)(2,1)S(1)} %collective-permute-done), channel_id=1, source_target_pairs={{0,2},{2,4},{4,6},{6,8},{8,10},{10,12},{12,14},{14,16},{16,18},{18... | collective-permute-start | bytes 589832 | tf_op jit(solution)/shard_map/ppermute | solution.py:17
  28.3 9.3 %collective-permute-start.2 = (bf16[48,2048]{1,0:T(8,128)(2,1)S(1)}, bf16[48,2048]{1,0:T(8,128)(2,1)S(1)}, u32[]{:S(2)}, u32[]{:S(2)}) collective-permute-start(bf16[48,2048]{1,0:T(8,128)(2,1)S(1)} %collective-permute-done.1), channel_id=1, source_target_pairs={{0,2},{2,4},{4,6},{6,8},{8,10},{10,12},{12,14},{14,16},{16,18},{18... | collective-permute-start | bytes 589832 | tf_op jit(solution)/shard_map/ppermute | solution.py:17
  37.6 9.3 %collective-permute-start.3 = (bf16[48,2048]{1,0:T(8,128)(2,1)S(1)}, bf16[48,2048]{1,0:T(8,128)(2,1)S(1)}, u32[]{:S(2)}, u32[]{:S(2)}) collective-permute-start(bf16[48,2048]{1,0:T(8,128)(2,1)S(1)} %collective-permute-done.2), channel_id=1, source_target_pairs={{0,2},{2,4},{4,6},{6,8},{8,10},{10,12},{12,14},{14,16},{16,18},{18... | collective-permute-start | bytes 589832 | tf_op jit(solution)/shard_map/ppermute | solution.py:17
  46.9 9.3 %collective-permute-start.4 = (bf16[48,2048]{1,0:T(8,128)(2,1)S(1)}, bf16[48,2048]{1,0:T(8,128)(2,1)S(1)}, u32[]{:S(2)}, u32[]{:S(2)}) collective-permute-start(bf16[48,2048]{1,0:T(8,128)(2,1)S(1)} %collective-permute-done.3), channel_id=1, source_target_pairs={{0,2},{2,4},{4,6},{6,8},{8,10},{10,12},{12,14},{14,16},{16,18},{18... | collective-permute-start | bytes 589832 | tf_op jit(solution)/shard_map/ppermute | solution.py:17
  56.1 9.3 %collective-permute-start.5 = (bf16[48,2048]{1,0:T(8,128)(2,1)S(1)}, bf16[48,2048]{1,0:T(8,128)(2,1)S(1)}, u32[]{:S(2)}, u32[]{:S(2)}) collective-permute-start(bf16[48,2048]{1,0:T(8,128)(2,1)S(1)} %collective-permute-done.4), channel_id=1, source_target_pairs={{0,2},{2,4},{4,6},{6,8},{8,10},{10,12},{12,14},{14,16},{16,18},{18... | collective-permute-start | bytes 589832 | tf_op jit(solution)/shard_map/ppermute | solution.py:17
  65.4 10.4 %collective-permute-start.6 = (bf16[48,2048]{1,0:T(8,128)(2,1)S(1)}, bf16[48,2048]{1,0:T(8,128)(2,1)S(1)}, u32[]{:S(2)}, u32[]{:S(2)}) collective-permute-start(bf16[48,2048]{1,0:T(8,128)(2,1)S(1)} %collective-permute-done.5), channel_id=1, source_target_pairs={{0,2},{2,4},{4,6},{6,8},{8,10},{10,12},{12,14},{14,16},{16,18},{18... | collective-permute-start | bytes 589832 | tf_op jit(solution)/shard_map/ppermute | solution.py:17
  75.8 11.2 %collective-permute-start.7 = (bf16[48,2048]{1,0:T(8,128)(2,1)S(1)}, bf16[48,2048]{1,0:T(8,128)(2,1)S(1)}, u32[]{:S(2)}, u32[]{:S(2)}) collective-permute-start(bf16[48,2048]{1,0:T(8,128)(2,1)S(1)} %collective-permute-done.6), channel_id=1, source_target_pairs={{0,2},{2,4},{4,6},{6,8},{8,10},{10,12},{12,14},{14,16},{16,18},{18... | collective-permute-start | bytes 589832 | tf_op jit(solution)/shard_map/ppermute | solution.py:17
  87.0 10.3 %collective-permute-start.8 = (bf16[48,2048]{1,0:T(8,128)(2,1)S(1)}, bf16[48,2048]{1,0:T(8,128)(2,1)S(1)}, u32[]{:S(2)}, u32[]{:S(2)}) collective-permute-start(bf16[48,2048]{1,0:T(8,128)(2,1)S(1)} %collective-permute-done.7), channel_id=1, source_target_pairs={{0,2},{2,4},{4,6},{6,8},{8,10},{10,12},{12,14},{14,16},{16,18},{18... | collective-permute-start | bytes 589832 | tf_op jit(solution)/shard_map/ppermute | solution.py:17
  97.3 9.5 %collective-permute-start.9 = (bf16[48,2048]{1,0:T(8,128)(2,1)S(1)}, bf16[48,2048]{1,0:T(8,128)(2,1)S(1)}, u32[]{:S(2)}, u32[]{:S(2)}) collective-permute-start(bf16[48,2048]{1,0:T(8,128)(2,1)S(1)} %collective-permute-done.8), channel_id=1, source_target_pairs={{0,2},{2,4},{4,6},{6,8},{8,10},{10,12},{12,14},{14,16},{16,18},{18... | collective-permute-start | bytes 589832 | tf_op jit(solution)/shard_map/ppermute | solution.py:17
  106.8 9.3 %collective-permute-start.10 = (bf16[48,2048]{1,0:T(8,128)(2,1)S(1)}, bf16[48,2048]{1,0:T(8,128)(2,1)S(1)}, u32[]{:S(2)}, u32[]{:S(2)}) collective-permute-start(bf16[48,2048]{1,0:T(8,128)(2,1)S(1)} %collective-permute-done.9), channel_id=1, source_target_pairs={{0,2},{2,4},{4,6},{6,8},{8,10},{10,12},{12,14},{14,16},{16,18},{18... | collective-permute-start | bytes 589832 | tf_op jit(solution)/shard_map/ppermute | solution.py:17
  116.1 9.3 %collective-permute-start.11 = (bf16[48,2048]{1,0:T(8,128)(2,1)S(1)}, bf16[48,2048]{1,0:T(8,128)(2,1)S(1)}, u32[]{:S(2)}, u32[]{:S(2)}) collective-permute-start(bf16[48,2048]{1,0:T(8,128)(2,1)S(1)} %collective-permute-done.10), channel_id=1, source_target_pairs={{0,2},{2,4},{4,6},{6,8},{8,10},{10,12},{12,14},{14,16},{16,18},{18... | collective-permute-start | bytes 589832 | tf_op jit(solution)/shard_map/ppermute | solution.py:17
  125.3 9.3 %collective-permute-start.12 = (bf16[48,2048]{1,0:T(8,128)(2,1)S(1)}, bf16[48,2048]{1,0:T(8,128)(2,1)S(1)}, u32[]{:S(2)}, u32[]{:S(2)}) collective-permute-start(bf16[48,2048]{1,0:T(8,128)(2,1)S(1)} %collective-permute-done.11), channel_id=1, source_target_pairs={{0,2},{2,4},{4,6},{6,8},{8,10},{10,12},{12,14},{14,16},{16,18},{18... | collective-permute-start | bytes 589832 | tf_op jit(solution)/shard_map/ppermute | solution.py:17
  134.6 9.3 %collective-permute-start.13 = (bf16[48,2048]{1,0:T(8,128)(2,1)S(1)}, bf16[48,2048]{1,0:T(8,128)(2,1)S(1)}, u32[]{:S(2)}, u32[]{:S(2)}) collective-permute-start(bf16[48,2048]{1,0:T(8,128)(2,1)S(1)} %collective-permute-done.12), channel_id=1, source_target_pairs={{0,2},{2,4},{4,6},{6,8},{8,10},{10,12},{12,14},{14,16},{16,18},{18... | collective-permute-start | bytes 589832 | tf_op jit(solution)/shard_map/ppermute | solution.py:17
  143.9 9.3 %collective-permute-start.14 = (bf16[48,2048]{1,0:T(8,128)(2,1)S(1)}, bf16[48,2048]{1,0:T(8,128)(2,1)S(1)}, u32[]{:S(2)}, u32[]{:S(2)}) collective-permute-start(bf16[48,2048]{1,0:T(8,128)(2,1)S(1)} %collective-permute-done.13), channel_id=1, source_target_pairs={{0,2},{2,4},{4,6},{6,8},{8,10},{10,12},{12,14},{14,16},{16,18},{18... | collective-permute-start | bytes 589832 | tf_op jit(solution)/shard_map/ppermute | solution.py:17
  143.9 10.9 %copy-start.4 = (f32[704,2048]{1,0:T(8,128)S(1)}, f32[704,2048]{1,0:T(8,128)}, u32[]{:S(2)}) copy-start(f32[704,2048]{1,0:T(8,128)} %param.11) | copy-start | bytes 17301508
  143.9 11.0 %copy-start.5 = (f32[2048]{0:T(1024)S(1)}, f32[2048]{0:T(1024)}, u32[]{:S(2)}) copy-start(f32[2048]{0:T(1024)} %param.10) | copy-start | bytes 24580
  154.8 5.1 %slice-start = ((s8[5767168]{0:T(1024)(128)(4,1)}), s8[4194304]{0:T(1024)(128)(4,1)S(1)}, s32[]{:S(2)}) async-start(s8[5767168]{0:T(1024)(128)(4,1)} %bitcast.4), calls=%async_computation.3 | async-start | bytes 8388608
  154.8 4.2 %copy-start.1 = (bf16[1536,2048]{1,0:T(8,128)(2,1)}, bf16[1536,2048]{1,0:T(8,128)(2,1)S(1)}, u32[]{:S(2)}) copy-start(bf16[1536,2048]{1,0:T(8,128)(2,1)S(1)} %constant_dynamic-update-slice_fusion) | copy-start | bytes 18874372
  154.8 5.6 %slice-start.1 = ((s8[5767168]{0:T(1024)(128)(4,1)}), s8[1572864]{0:T(1024)(128)(4,1)S(1)}, s32[]{:S(2)}) async-start(s8[5767168]{0:T(1024)(128)(4,1)} %bitcast.4), calls=%async_computation.4 | async-start | bytes 3145728
  164.3 24.5 %copy-start.6 = (f32[704]{0:T(1024)S(1)}, f32[704]{0:T(1024)}, u32[]{:S(2)}) copy-start(f32[704]{0:T(1024)} %param.14) | copy-start | bytes 8452
  164.3 24.5 %copy-start.7 = (f32[704]{0:T(1024)S(1)}, f32[704]{0:T(1024)}, u32[]{:S(2)}) copy-start(f32[704]{0:T(1024)} %param.12) | copy-start | bytes 8452
  164.3 182.1 %reduce-scatter.2.cloned.1.call-start = ((), (), s32[]{:S(2)}) async-start(), calls=%async_computation.1 | async-start | bytes 6684672 | tf_op jit(solution)/shard_map/reduce_scatter | solution.py:54
  198.2 148.2 %copy-start.2 = (f32[2048]{0:T(1024)S(1)}, f32[2048]{0:T(1024)}, u32[]{:S(2)}) copy-start(f32[2048]{0:T(1024)} %param.16) | copy-start | bytes 24580
  198.2 151.8 %copy-start.3 = (f32[2048]{0:T(1024)S(1)}, f32[2048]{0:T(1024)}, u32[]{:S(2)}) copy-start(f32[2048]{0:T(1024)} %param.17) | copy-start | bytes 24580
Sparse Core Ops, SparseCore 0:
  164.4 24.2 all-reduce.2
  198.4 147.9 reduce-scatter.1
